TPU v7x, 32 devices: a whole 2x2x4 slice. The times are simulated.
32 devices in a mesh: fs: 8 (over z, x), tp: 4 (over y, core).
Axes of the slice: x: 2, y: 2, z: 4, core: 2. Of those that a mesh axis runs over, the one named last changes fastest.
Arguments:
- normed_inputs: bfloat16 [24576, 2048], P(('fs', 'tp')), may hold values from -6 to 6
- query_cotangent: bfloat16 [24576, 1024], P(('fs', 'tp')), may hold values from -6 to 6
- head_outputs: bfloat16 [24576, 1024], P(('fs', 'tp')), may hold values from -6 to 6
- output_cotangent: bfloat16 [24576, 2048], P(('fs', 'tp')), may hold values from -6 to 6
- query_weight: float32 [2048, 1024], P('fs', 'tp'), may hold values from -0.125 to 0.125
- out_weight: float32 [1024, 2048], P('fs', 'tp'), may hold values from -0.1875 to 0.1875
- query_basis: bfloat16 [2048, 512], P('fs'), may hold values from -0.125 to 0.125
- out_basis: bfloat16 [1024, 512], P('fs'), may hold values from -0.1875 to 0.1875
- query_mean: float32 [512, 1024], P('fs', 'tp'), may hold values from -6 to 6
- query_square: float32 [512, 1024], P('fs', 'tp'), may hold values from 0.5 to 2
- out_mean: float32 [512, 2048], P('fs', 'tp'), may hold values from -6 to 6
- out_square: float32 [512, 2048], P('fs', 'tp'), may hold values from 0.5 to 2
Outputs:
- query_mean_new: float32 [512, 1024], P('fs', 'tp')
- query_square_new: float32 [512, 1024], P('fs', 'tp')
- query_step: float32 [2048, 1024], P('fs', 'tp')
- query_weight_new: float32 [2048, 1024], P('fs', 'tp')
- query_copy: bfloat16 [2048, 1024], P(None, 'tp')
- out_mean_new: float32 [512, 2048], P('fs', 'tp')
- out_square_new: float32 [512, 2048], P('fs', 'tp')
- out_step: float32 [1024, 2048], P('fs', 'tp')
- out_weight_new: float32 [1024, 2048], P('fs', 'tp')
- out_copy: bfloat16 [1024, 2048], P(None, 'tp')
All inputs are finite; a program needn't handle non-finite values.
Results may differ from a plain program's by a relative error of at most 0.009.
Values may be sent and summed in bfloat16 or wider, within the bound.
No kernel may reach another device: no remote copies, remote signals or barrier semaphores. Data moves between devices by JAX's collectives and lax.ppermute only.
A program may use at most 64 MiB of HBM per device.

v0:
```python
import jax
import jax.numpy as jnp
from jax import lax
from jax.sharding import PartitionSpec as P


def moments(reduced, mean, square):
    mean_new = 0.8 * mean + 0.2 * reduced
    square_new = 0.9 * square + 0.1 * reduced * reduced
    direction = mean_new / (jnp.sqrt(square_new) + 1e-08)
    return (mean_new, square_new, direction)


def split_product(left, right):
    contract = (((0,), (0,)), ((), ()))
    high = left.astype(jnp.bfloat16)
    low = (left - high.astype(jnp.float32)).astype(jnp.bfloat16)
    return lax.dot_general(
        high, right, contract, preferred_element_type=jnp.float32
    ) + lax.dot_general(low, right, contract, preferred_element_type=jnp.float32)


def shards(
    normed_inputs,
    query_cotangent,
    head_outputs,
    output_cotangent,
    query_weight,
    out_weight,
    query_basis,
    out_basis,
    query_mean,
    query_square,
    out_mean,
    out_square,
):
    fs_count = lax.axis_size("fs")
    tp_count = lax.axis_size("tp")
    model_rows = normed_inputs.shape[1]
    query_width = query_cotangent.shape[1]
    token_scale = (normed_inputs.shape[0] * fs_count * tp_count) ** (-0.5)
    query_cols = query_weight.shape[1]
    out_cols = out_weight.shape[1]
    rank_rows = query_mean.shape[0]
    query_all, out_all = (
        lax.all_gather(query_basis, "fs", axis=0, tiled=True),
        lax.all_gather(out_basis, "fs", axis=0, tiled=True),
    )
    query_left = jnp.dot(normed_inputs, query_all, preferred_element_type=jnp.float32)
    out_left = jnp.dot(head_outputs, out_all, preferred_element_type=jnp.float32)
    query_part = split_product(query_left, query_cotangent)
    out_part = split_product(out_left, output_cotangent)
    reduced = lax.psum_scatter(
        jnp.concatenate(
            [
                query_part.reshape(rank_rows * lax.axis_size("fs"), tp_count, query_cols),
                out_part.reshape(rank_rows * lax.axis_size("fs"), tp_count, out_cols),
            ],
            axis=2,
        ).astype(jnp.bfloat16),
        "fs",
        scatter_dimension=0,
        tiled=True,
    )
    summed = lax.psum_scatter(reduced, "tp", scatter_dimension=1, tiled=True).astype(jnp.float32)
    projected = summed[:, 0, :]
    projected = projected * token_scale
    query_reduced = projected[:, :query_cols]
    out_reduced = projected[:, query_cols:]
    query_mean_new, query_square_new, query_direction = moments(
        query_reduced, query_mean, query_square
    )
    out_mean_new, out_square_new, out_direction = moments(out_reduced, out_mean, out_square)
    query_piece = lax.all_gather(query_direction, "fs", axis=0, tiled=True)
    out_piece = lax.all_gather(out_direction, "fs", axis=0, tiled=True)
    query_part = query_basis.astype(jnp.float32)
    out_part = out_basis.astype(jnp.float32)
    query_full = jnp.dot(query_part, query_piece, precision=lax.Precision.HIGHEST)
    out_full = jnp.dot(out_part, out_piece, precision=lax.Precision.HIGHEST)
    query_norms, out_norms = lax.psum(
        (jnp.sum(query_full * query_full, axis=0), jnp.sum(out_full * out_full, axis=0)), "fs"
    )
    query_step = query_full * lax.rsqrt(query_norms / model_rows + 0.05)
    out_step = out_full * lax.rsqrt(out_norms / query_width + 0.05)
    query_weight_new = query_weight - 0.01 * query_step
    out_weight_new = out_weight - 0.01 * out_step
    query_copy, out_copy = (
        lax.all_gather(query_weight_new.astype(jnp.bfloat16), "fs", axis=0, tiled=True),
        lax.all_gather(out_weight_new.astype(jnp.bfloat16), "fs", axis=0, tiled=True),
    )
    return (
        query_mean_new,
        query_square_new,
        query_step,
        query_weight_new,
        query_copy,
        out_mean_new,
        out_square_new,
        out_step,
        out_weight_new,
        out_copy,
    )


def solution(mesh):
    in_specs = (
        P(("fs", "tp"), None),
        P(("fs", "tp"), None),
        P(("fs", "tp"), None),
        P(("fs", "tp"), None),
        P("fs", "tp"),
        P("fs", "tp"),
        P("fs", None),
        P("fs", None),
        P("fs", "tp"),
        P("fs", "tp"),
        P("fs", "tp"),
        P("fs", "tp"),
    )
    out_specs = (
        P("fs", "tp"),
        P("fs", "tp"),
        P("fs", "tp"),
        P("fs", "tp"),
        P(None, "tp"),
        P("fs", "tp"),
        P("fs", "tp"),
        P("fs", "tp"),
        P("fs", "tp"),
        P(None, "tp"),
    )
    return jax.shard_map(shards, mesh=mesh, in_specs=in_specs, out_specs=out_specs, check_vma=False)
```

profile of v0, /device:TPU:0, one launch (start us, length us, event | category | flops | bytes accessed | tf_op | source)
XLA Modules:
  0.0 366.5 jit_solution(16840274893185502602)
XLA Ops:
  7.2 0.0 copy-start
  7.2 0.0 all-gather.8.cloned.1.call-start
  7.2 0.7 all-gather.8.cloned.1.call-update
  7.9 0.0 all-gather.6.cloned.1.call-start
  8.0 0.7 all-gather.6.cloned.1.call-update
  8.7 0.0 reduce-scatter.3.cloned.1.call-start
  8.7 44.4 %all-gather.8.cloned.1.call-done = bf16[1024,512]{1,0:T(8,128)(2,1)} async-done(((bf16[128,512]{1,0:T(8,128)(2,1)}), bf16[1024,512]{1,0:T(8,128)(2,1)}) %all-gather.8.cloned.1.call-update) | async-done | bytes 1048592 | tf_op jit(solution)/shard_map/all_gather | solution.py:47
  53.2 2.7 fusion.13
  55.8 0.0 copy-done
  55.8 1.8 fusion.1
  57.7 1.8 add_convert_fusion
  59.5 1.5 copy.28
  61.0 42.1 %all-gather.6.cloned.1.call-done = bf16[2048,512]{1,0:T(8,128)(2,1)} async-done(((bf16[256,512]{1,0:T(8,128)(2,1)}), bf16[2048,512]{1,0:T(8,128)(2,1)}) %all-gather.6.cloned.1.call-update) | async-done | bytes 2097168 | tf_op jit(solution)/shard_map/all_gather | solution.py:46
  103.1 4.4 %fusion.12 = f32[768,512]{1,0:T(8,128)S(1)} fusion(bf16[768,2048]{1,0:T(8,128)(2,1)} %param.12, bf16[2048,512]{1,0:T(8,128)(2,1)} %all-gather.6.cloned.1.call-done), kind=kOutput, calls=%fused_computation.32 | convolution fusion | flops 1610612736 | bytes 6815744 | tf_op jit(solution)/shard_map/dot_general | solution.py:49
  107.6 0.0 copy-done.7
  107.6 1.0 fusion.4
  108.6 1.0 add_convert_fusion.1
  109.6 0.1 copy.29
  109.7 1.5 copy-done.1
  111.2 1.9 pad_maximum_fusion
  113.0 0.0 reduce-scatter.3.cloned.1.call-update
  113.1 0.0 copy-start.6
  113.1 0.0 reduce-scatter.5.cloned.1.call-start
  113.1 73.1 %reduce-scatter.3.cloned.1.call-done = bf16[64,4,768]{2,0,1:T(8,128)(2,1)} async-done(((bf16[512,4,768]{2,0,1:T(8,128)(2,1)}), bf16[64,4,768]{2,0,1:T(8,128)(2,1)}) %reduce-scatter.3.cloned.1.call-update) | async-done | bytes 393232 | tf_op jit(solution)/shard_map/reduce_scatter | solution.py:53
  186.2 0.0 reduce-scatter.5.cloned.1.call-update
  186.2 0.0 all-gather.12.cloned.1.call-start
  186.3 22.2 %reduce-scatter.5.cloned.1.call-done = bf16[64,1,768]{2,0,1:T(8,128)(2,1)} async-done(((bf16[64,4,768]{2,0,1:T(8,128)(2,1)}), bf16[64,1,768]{2,0,1:T(8,128)(2,1)}) %reduce-scatter.5.cloned.1.call-update) | async-done | bytes 98320 | tf_op jit(solution)/shard_map/reduce_scatter | solution.py:65
  208.5 0.9 multiply_bitcast_fusion.2
  209.4 0.0 copy-start.5
  209.4 0.7 copy-done.5
  210.1 1.7 add_divide_fusion
  211.8 0.0 all-gather.12.cloned.1.call-update
  211.9 0.0 all-gather.14.cloned.1.call-start
  211.9 1.6 add_divide_fusion.1
  213.5 32.6 %all_gather.20 = f32[512,256]{1,0:T(8,128)S(1)} all-gather(f32[64,256]{1,0:T(8,128)S(1)} %get-tuple-element.21), channel_id=1, replica_groups=mesh['fs'=8,'tp'=4] {'fs'}, dimensions={0}, use_global_device_ids=true | all-gather | bytes 589824 | tf_op jit(solution)/shard_map/all_gather | solution.py:74
  246.1 1.1 multiply_reduce_fusion.1
  247.2 6.5 %all-gather.12.cloned.1.call-done = f32[512,512]{1,0:T(8,128)} async-done(((f32[64,512]{1,0:T(8,128)}), f32[512,512]{1,0:T(8,128)}) %all-gather.12.cloned.1.call-update) | async-done | bytes 1048592 | tf_op jit(solution)/shard_map/all_gather | solution.py:75
  253.7 2.4 multiply_reduce_fusion
  256.2 19.1 %all-reduce = (f32[256]{0:T(256)S(1)}, f32[512]{0:T(512)S(1)}) all-reduce(f32[256]{0:T(256)S(1)} %get-tuple-element.24, f32[512]{0:T(512)S(1)} %get-tuple-element.26), channel_id=1, replica_groups=mesh['fs'=8,'tp'=4] {'fs'}, use_global_device_ids=true, to_apply=%region_3.0 | all-reduce | flops 768 | bytes 6144 | tf_op jit(solution)/shard_map/psum | solution.py:80
  275.2 1.9 fusion.8
  277.2 0.0 all-gather.14.cloned.1.call-update
  277.2 0.0 all-gather.10.cloned.1.call-start
  277.3 1.8 fusion.9
  279.1 0.0 all-gather.10.cloned.1.call-update
  279.1 35.5 %all-gather.14.cloned.1.call-done = bf16[1024,512]{1,0:T(8,128)(2,1)} async-done(((bf16[128,512]{1,0:T(8,128)(2,1)}), bf16[1024,512]{1,0:T(8,128)(2,1)}) %all-gather.14.cloned.1.call-update) | async-done | bytes 1048592 | tf_op jit(solution)/shard_map/all_gather | solution.py:89
  314.7 41.7 %all-gather.10.cloned.1.call-done = bf16[2048,256]{1,0:T(8,128)(2,1)} async-done(((bf16[256,256]{1,0:T(8,128)(2,1)}), bf16[2048,256]{1,0:T(8,128)(2,1)}) %all-gather.10.cloned.1.call-update) | async-done | bytes 1048592 | tf_op jit(solution)/shard_map/all_gather | solution.py:88
  356.4 2.4 copy.32
  358.7 1.0 copy.33
  (11 shorter events, 0.0 us)
Async XLA Ops:
  7.2 48.7 %copy-start = (bf16[768,2048]{1,0:T(8,128)(2,1)S(1)}, bf16[768,2048]{1,0:T(8,128)(2,1)}, u32[]{:S(2)}) copy-start(bf16[768,2048]{1,0:T(8,128)(2,1)} %param.15) | copy-start | bytes 9437188
  7.2 46.0 %all-gather.8.cloned.1.call-start = ((), (), s32[]{:S(2)}) async-start(), calls=%async_computation.3 | async-start | bytes 1179648 | tf_op jit(solution)/shard_map/all_gather | solution.py:47
  7.9 95.2 %all-gather.6.cloned.1.call-start = ((), (), s32[]{:S(2)}) async-start(), calls=%async_computation.2 | async-start | bytes 2359296 | tf_op jit(solution)/shard_map/all_gather | solution.py:46
  8.7 177.5 %reduce-scatter.3.cloned.1.call-start = ((), (), s32[]{:S(2)}) async-start(), calls=%async_computation.4 | async-start | bytes 3538944 | tf_op jit(solution)/shard_map/reduce_scatter | solution.py:53
  103.1 4.4 %copy-start.7 = (bf16[768,1024]{1,0:T(8,128)(2,1)S(1)}, bf16[768,1024]{1,0:T(8,128)(2,1)}, u32[]{:S(2)}) copy-start(bf16[768,1024]{1,0:T(8,128)(2,1)} %param.13) | copy-start | bytes 4718596
  109.6 1.6 copy-start.1
  113.0 133.0 %copy-start.2 = (bf16[256,512]{1,0:T(8,128)(2,1)S(1)}, bf16[256,512]{1,0:T(8,128)(2,1)}, u32[]{:S(2)}) copy-start(bf16[256,512]{1,0:T(8,128)(2,1)} %param.18) | copy-start | bytes 786436
  113.1 140.7 %copy-start.6 = (bf16[128,512]{1,0:T(8,128)(2,1)S(1)}, bf16[128,512]{1,0:T(8,128)(2,1)}, u32[]{:S(2)}) copy-start(bf16[128,512]{1,0:T(8,128)(2,1)} %param.19) | copy-start | bytes 393220
  113.1 95.4 %reduce-scatter.5.cloned.1.call-start = ((), (), s32[]{:S(2)}) async-start(), calls=%async_computation.5 | async-start | bytes 491520 | tf_op jit(solution)/shard_map/reduce_scatter | solution.py:65
  186.2 67.5 %all-gather.12.cloned.1.call-start = ((), (), s32[]{:S(2)}) async-start(), calls=%async_computation.7 | async-start | bytes 1179648 | tf_op jit(solution)/shard_map/all_gather | solution.py:75
  209.4 0.7 copy-start.5
  211.9 102.8 %all-gather.14.cloned.1.call-start = ((), (), s32[]{:S(2)}) async-start(), calls=%async_computation.8 | async-start | bytes 1179648 | tf_op jit(solution)/shard_map/all_gather | solution.py:89
  247.2 30.1 %copy-start.4 = (f32[256,256]{0,1:T(8,128)S(1)}, f32[256,256]{0,1:T(8,128)}, u32[]{:S(2)}) copy-start(f32[256,256]{0,1:T(8,128)} %get-tuple-element.25) | copy-start | bytes 786436
  277.2 79.2 %all-gather.10.cloned.1.call-start = ((), (), s32[]{:S(2)}) async-start(), calls=%async_computation.6 | async-start | bytes 1179648 | tf_op jit(solution)/shard_map/all_gather | solution.py:88
  356.4 2.4 copy-start.3
Sparse Core Ops, SparseCore 0:
  10.1 42.9 all-gather.7
  55.3 47.7 all-gather.5
  113.2 72.9 reduce-scatter.2
  188.5 19.9 reduce-scatter.4
  212.0 41.7 all-gather.11
  277.3 37.2 all-gather.13
  317.3 38.9 all-gather.9
where the time goes:
time: 367 us
  waiting for transfers between devices  267 us (73%)
  blocking collectives  51.6 us (14%)
  matrix products  16.4 us (4%)
  between operations  14.2 us (4%)
  other arithmetic  9.87 us (3%)
  local copies, waits for them, and re-layouts  7.1 us (2%)
    reduce_scatter x1, waiting for transfers between devices, shards(): lax.psum_scatter(jnp.concatenate([query_part.reshape(rank_rows * lax.axis...  73.1 us
    all_gather x1, waiting for transfers between devices, shards(): lax.all_gather(out_basis, 'fs', axis=0, tiled=True)  44.4 us
    all_gather x1, waiting for transfers between devices, shards(): lax.all_gather(query_basis, 'fs', axis=0, tiled=True)  42.1 us
    all_gather x1, waiting for transfers between devices, shards(): lax.all_gather(query_weight_new.astype(jnp.bfloat16), 'fs', axis=0, tiled...  41.7 us
    all_gather x1, waiting for transfers between devices, shards(): lax.all_gather(out_weight_new.astype(jnp.bfloat16), 'fs', axis=0, tiled=T...  35.5 us
    all_gather x1, blocking collectives, shards(): query_piece = lax.all_gather(query_direction, 'fs', axis=0, tiled=True)  32.6 us
    reduce_scatter x1, waiting for transfers between devices, shards(): lax.psum_scatter(reduced, 'tp', scatter_dimension=1, tiled=True)  22.2 us
    psum x1, blocking collectives, shards(): lax.psum((jnp.sum(query_full * query_full, axis=0), jnp.sum(out_full * ou...  19.1 us
  transfers between devices with their start and end apart: 7, of which 7 were waited for; matrix products, arithmetic and copies ran while one was open for 3% of the time, Pallas kernels for 0%

commit v1 on v0

--- a/solution.py
+++ b/solution.py
@@ -71,8 +71,13 @@
         query_reduced, query_mean, query_square
     )
     out_mean_new, out_square_new, out_direction = moments(out_reduced, out_mean, out_square)
-    query_piece = lax.all_gather(query_direction, "fs", axis=0, tiled=True)
-    out_piece = lax.all_gather(out_direction, "fs", axis=0, tiled=True)
+    query_piece, out_piece = jnp.split(
+        lax.all_gather(
+            jnp.concatenate([query_direction, out_direction], axis=1), "fs", axis=0, tiled=True
+        ),
+        [query_direction.shape[1]],
+        axis=1,
+    )
     query_part = query_basis.astype(jnp.float32)
     out_part = out_basis.astype(jnp.float32)
     query_full = jnp.dot(query_part, query_piece, precision=lax.Precision.HIGHEST)

time: 367 us -> 373 us (1.016)
  waiting for transfers between devices: 267 us -> 305 us
  blocking collectives: 51.6 us -> 18.8 us
    all_gather x1, waiting for transfers between devices: 6.53 us -> 44.3 us  [shards(): lax.all_gather(jnp.concatenate([query_direction, out_direction], axis=1),...]
    all_gather x1 -> x0, blocking collectives: 32.6 us -> none  [shards(): query_piece = lax.all_gather(query_direction, 'fs', axis=0, tiled=True)]
where the time goes in v1:
time: 373 us
  waiting for transfers between devices  305 us (82%)
  blocking collectives  18.8 us (5%)
  matrix products  17.4 us (5%)
  between operations  14.2 us (4%)
  other arithmetic  10.6 us (3%)
  local copies, waits for them, and re-layouts  6.44 us (2%)
    reduce_scatter x1, waiting for transfers between devices, shards(): lax.psum_scatter(jnp.concatenate([query_part.reshape(rank_rows * lax.axis...  73.1 us
    all_gather x1, waiting for transfers between devices, shards(): lax.all_gather(out_basis, 'fs', axis=0, tiled=True)  44.4 us
    all_gather x1, waiting for transfers between devices, shards(): lax.all_gather(jnp.concatenate([query_direction, out_direction], axis=1),...  44.3 us
    all_gather x1, waiting for transfers between devices, shards(): lax.all_gather(query_basis, 'fs', axis=0, tiled=True)  42.1 us
    all_gather x1, waiting for transfers between devices, shards(): lax.all_gather(query_weight_new.astype(jnp.bfloat16), 'fs', axis=0, tiled...  41.7 us
    all_gather x1, waiting for transfers between devices, shards(): lax.all_gather(out_weight_new.astype(jnp.bfloat16), 'fs', axis=0, tiled=T...  35.7 us
    reduce_scatter x1, waiting for transfers between devices, shards(): lax.psum_scatter(reduced, 'tp', scatter_dimension=1, tiled=True)  22.2 us
    psum x1, blocking collectives, shards(): lax.psum((jnp.sum(query_full * query_full, axis=0), jnp.sum(out_full * ou...  18.8 us
  transfers between devices with their start and end apart: 7, of which 7 were waited for; matrix products, arithmetic and copies ran while one was open for 3% of the time, Pallas kernels for 0%

profile of v1, /device:TPU:0, one launch (start us, length us, event | category | flops | bytes accessed | tf_op | source)
XLA Modules:
  0.0 372.6 jit_solution(12111795478647899167)
XLA Ops:
  7.2 0.0 copy-start
  7.2 0.0 all-gather.8.cloned.1.call-start
  7.2 0.7 all-gather.8.cloned.1.call-update
  7.9 0.0 all-gather.6.cloned.1.call-start
  8.0 0.7 all-gather.6.cloned.1.call-update
  8.7 0.0 reduce-scatter.3.cloned.1.call-start
  8.7 44.4 %all-gather.8.cloned.1.call-done = bf16[1024,512]{1,0:T(8,128)(2,1)} async-done(((bf16[128,512]{1,0:T(8,128)(2,1)}), bf16[1024,512]{1,0:T(8,128)(2,1)}) %all-gather.8.cloned.1.call-update) | async-done | bytes 1048592 | tf_op jit(solution)/shard_map/all_gather | solution.py:47
  53.2 2.7 fusion.17
  55.8 0.0 copy-done
  55.8 1.8 fusion.5
  57.7 1.8 add_convert_fusion
  59.5 1.5 copy.28
  61.0 42.1 %all-gather.6.cloned.1.call-done = bf16[2048,512]{1,0:T(8,128)(2,1)} async-done(((bf16[256,512]{1,0:T(8,128)(2,1)}), bf16[2048,512]{1,0:T(8,128)(2,1)}) %all-gather.6.cloned.1.call-update) | async-done | bytes 2097168 | tf_op jit(solution)/shard_map/all_gather | solution.py:46
  103.1 4.4 %fusion.16 = f32[768,512]{1,0:T(8,128)S(1)} fusion(bf16[768,2048]{1,0:T(8,128)(2,1)} %param.12, bf16[2048,512]{1,0:T(8,128)(2,1)} %all-gather.6.cloned.1.call-done), kind=kOutput, calls=%fused_computation.37 | convolution fusion | flops 1610612736 | bytes 6815744 | tf_op jit(solution)/shard_map/dot_general | solution.py:49
  107.6 0.0 copy-done.5
  107.6 1.0 fusion.8
  108.6 1.0 add_convert_fusion.1
  109.6 0.0 copy-start.1
  109.6 0.1 copy.29
  109.7 1.5 copy-done.1
  111.2 1.8 pad_maximum_fusion
  113.0 0.0 reduce-scatter.3.cloned.1.call-update
  113.1 0.0 copy-start.2
  113.1 0.0 reduce-scatter.5.cloned.1.call-start
  113.1 73.1 %reduce-scatter.3.cloned.1.call-done = bf16[64,4,768]{2,0,1:T(8,128)(2,1)} async-done(((bf16[512,4,768]{2,0,1:T(8,128)(2,1)}), bf16[64,4,768]{2,0,1:T(8,128)(2,1)}) %reduce-scatter.3.cloned.1.call-update) | async-done | bytes 393232 | tf_op jit(solution)/shard_map/reduce_scatter | solution.py:53
  186.2 0.0 reduce-scatter.5.cloned.1.call-update
  186.2 0.0 all-gather.10.cloned.1.call-start
  186.3 22.2 %reduce-scatter.5.cloned.1.call-done = bf16[64,1,768]{2,0,1:T(8,128)(2,1)} async-done(((bf16[64,4,768]{2,0,1:T(8,128)(2,1)}), bf16[64,1,768]{2,0,1:T(8,128)(2,1)}) %reduce-scatter.5.cloned.1.call-update) | async-done | bytes 98320 | tf_op jit(solution)/shard_map/reduce_scatter | solution.py:65
  208.5 0.9 multiply_bitcast_fusion.2
  209.4 1.7 add_divide_fusion
  211.1 1.6 add_divide_fusion.1
  212.7 0.7 pad_maximum_fusion.1
  213.4 0.0 all-gather.10.cloned.1.call-update
  213.4 0.0 all-gather.14.cloned.1.call-start
  213.5 44.3 %all-gather.10.cloned.1.call-done = f32[512,768]{1,0:T(8,128)} async-done(((f32[64,768]{1,0:T(8,128)}), f32[512,768]{1,0:T(8,128)}) %all-gather.10.cloned.1.call-update) | async-done | bytes 1572880 | tf_op jit(solution)/shard_map/all_gather | solution.py:75
  257.7 2.4 multiply_reduce_fusion
  260.2 0.0 copy-done.2
  260.2 2.2 multiply_reduce_fusion.1
  262.3 18.8 %all-reduce = (f32[256]{0:T(256)S(1)}, f32[512]{0:T(512)S(1)}) all-reduce(f32[256]{0:T(256)S(1)} %get-tuple-element.24, f32[512]{0:T(512)S(1)} %get-tuple-element.26), channel_id=1, replica_groups=mesh['fs'=8,'tp'=4] {'fs'}, use_global_device_ids=true, to_apply=%region_3.0 | all-reduce | flops 768 | bytes 6144 | tf_op jit(solution)/shard_map/psum | solution.py:85
  281.1 1.9 fusion.12
  283.1 0.0 all-gather.14.cloned.1.call-update
  283.1 0.0 all-gather.12.cloned.1.call-start
  283.2 1.9 fusion.13
  285.1 0.0 all-gather.12.cloned.1.call-update
  285.1 35.7 %all-gather.14.cloned.1.call-done = bf16[1024,512]{1,0:T(8,128)(2,1)} async-done(((bf16[128,512]{1,0:T(8,128)(2,1)}), bf16[1024,512]{1,0:T(8,128)(2,1)}) %all-gather.14.cloned.1.call-update) | async-done | bytes 1048592 | tf_op jit(solution)/shard_map/all_gather | solution.py:94
  320.8 41.7 %all-gather.12.cloned.1.call-done = bf16[2048,256]{1,0:T(8,128)(2,1)} async-done(((bf16[256,256]{1,0:T(8,128)(2,1)}), bf16[2048,256]{1,0:T(8,128)(2,1)}) %all-gather.12.cloned.1.call-update) | async-done | bytes 1048592 | tf_op jit(solution)/shard_map/all_gather | solution.py:93
  362.5 2.4 copy.32
  364.8 1.0 copy.33
  (7 shorter events, 0.0 us)
Async XLA Ops:
  7.2 48.7 %copy-start = (bf16[768,2048]{1,0:T(8,128)(2,1)S(1)}, bf16[768,2048]{1,0:T(8,128)(2,1)}, u32[]{:S(2)}) copy-start(bf16[768,2048]{1,0:T(8,128)(2,1)} %param.15) | copy-start | bytes 9437188
  7.2 46.0 %all-gather.8.cloned.1.call-start = ((), (), s32[]{:S(2)}) async-start(), calls=%async_computation.3 | async-start | bytes 1179648 | tf_op jit(solution)/shard_map/all_gather | solution.py:47
  7.9 95.2 %all-gather.6.cloned.1.call-start = ((), (), s32[]{:S(2)}) async-start(), calls=%async_computation.2 | async-start | bytes 2359296 | tf_op jit(solution)/shard_map/all_gather | solution.py:46
  8.7 177.5 %reduce-scatter.3.cloned.1.call-start = ((), (), s32[]{:S(2)}) async-start(), calls=%async_computation.4 | async-start | bytes 3538944 | tf_op jit(solution)/shard_map/reduce_scatter | solution.py:53
  103.1 4.4 %copy-start.5 = (bf16[768,1024]{1,0:T(8,128)(2,1)S(1)}, bf16[768,1024]{1,0:T(8,128)(2,1)}, u32[]{:S(2)}) copy-start(bf16[768,1024]{1,0:T(8,128)(2,1)} %param.13) | copy-start | bytes 4718596
  109.6 1.6 copy-start.1
  113.0 144.7 %copy-start.4 = (bf16[128,512]{1,0:T(8,128)(2,1)S(1)}, bf16[128,512]{1,0:T(8,128)(2,1)}, u32[]{:S(2)}) copy-start(bf16[128,512]{1,0:T(8,128)(2,1)} %param.19) | copy-start | bytes 393220
  113.1 147.1 %copy-start.2 = (bf16[256,512]{1,0:T(8,128)(2,1)S(1)}, bf16[256,512]{1,0:T(8,128)(2,1)}, u32[]{:S(2)}) copy-start(bf16[256,512]{1,0:T(8,128)(2,1)} %param.18) | copy-start | bytes 786436
  113.1 95.4 %reduce-scatter.5.cloned.1.call-start = ((), (), s32[]{:S(2)}) async-start(), calls=%async_computation.5 | async-start | bytes 491520 | tf_op jit(solution)/shard_map/reduce_scatter | solution.py:65
  186.2 71.5 %all-gather.10.cloned.1.call-start = ((), (), s32[]{:S(2)}) async-start(), calls=%async_computation.6 | async-start | bytes 1769472 | tf_op jit(solution)/shard_map/all_gather | solution.py:75
  213.4 107.3 %all-gather.14.cloned.1.call-start = ((), (), s32[]{:S(2)}) async-start(), calls=%async_computation.8 | async-start | bytes 1179648 | tf_op jit(solution)/shard_map/all_gather | solution.py:94
  283.1 79.4 %all-gather.12.cloned.1.call-start = ((), (), s32[]{:S(2)}) async-start(), calls=%async_computation.7 | async-start | bytes 1179648 | tf_op jit(solution)/shard_map/all_gather | solution.py:93
  362.5 2.4 copy-start.3
Sparse Core Ops, SparseCore 0:
  10.1 42.9 all-gather.7
  55.3 47.7 all-gather.5
  113.2 72.9 reduce-scatter.2
  188.5 19.9 reduce-scatter.4
  213.5 44.1 all-gather.9
  283.2 37.4 all-gather.13
  323.5 38.9 all-gather.11
